TPU v7x, 32 devices: a whole 2x2x4 slice. The times are simulated.
32 devices in a mesh: sp: 16 (over z, y, x), tp: 2 (over core).
Axes of the slice: x: 2, y: 2, z: 4, core: 2. Of those that a mesh axis runs over, the one named last changes fastest.
Arguments:
- target: bfloat16 [4096, 1024], P(('sp', 'tp')), may hold values from -60 to 60
- source: bfloat16 [2048, 1024], P('sp'), may hold values from -7 to 7
- target_gains: bfloat16 [2, 4, 1024], replicated, may hold values from 0.099609375 to 1.8984375
- source_gain: bfloat16 [2, 1024], replicated, may hold values from 0.099609375 to 1.8984375
- query_weight: bfloat16 [2, 1024, 1024], P(None, None, 'tp'), may hold values from -0.1875 to 0.1875
- key_weight: bfloat16 [2, 1024, 1024], P(None, None, 'tp'), may hold values from -7.5625 to 7.5625
- value_weight: bfloat16 [2, 1024, 1024], P(None, None, 'tp'), may hold values from -0.1875 to 0.1875
- out_weight: bfloat16 [2, 1024, 1024], P(None, 'tp'), may hold values from -0.1875 to 0.1875
- gate_weight: bfloat16 [2, 1024, 1536], P(None, None, 'tp'), may hold values from -0.1875 to 0.1875
- up_weight: bfloat16 [2, 1024, 1536], P(None, None, 'tp'), may hold values from -0.1875 to 0.1875
- down_weight: bfloat16 [2, 1536, 1024], P(None, 'tp'), may hold values from -0.15625 to 0.15625
Outputs:
- stream: bfloat16 [4096, 1024], P(('sp', 'tp'))
All inputs are finite; a program needn't handle non-finite values.
Results may differ from a plain program's by a relative error of at most 0.04.
Values may be sent and summed in bfloat16 or wider, within the bound.
A program may use at most 64 MiB of HBM per device.

v0:
```python
import jax
import jax.numpy as jnp
from jax import lax
from jax.sharding import PartitionSpec as P

HEAD_DIM = 128


epsilon = 1e-06


def rms_norm(values, gain_row):
    widened = values.astype(jnp.float32)
    inverse = lax.rsqrt(jnp.mean(widened * widened, axis=-1, keepdims=True) + epsilon)
    return widened * inverse * gain_row.astype(jnp.float32)


def per_device(
    target,
    source,
    target_gains,
    source_gain,
    query_weight,
    key_weight,
    value_weight,
    out_weight,
    gate_weight,
    up_weight,
    down_weight,
):
    layers = query_weight.shape[0]
    own_rows = target.shape[0]
    heads_dev = query_weight.shape[2] // HEAD_DIM
    factor = HEAD_DIM ** (-0.5)

    def source_heads(layer_index):
        normed_source = rms_norm(source, source_gain[layer_index]).astype(jnp.bfloat16)
        key_rows = jnp.dot(
            normed_source, key_weight[layer_index], preferred_element_type=jnp.float32
        ).astype(jnp.bfloat16)
        value_rows = jnp.dot(
            normed_source, value_weight[layer_index], preferred_element_type=jnp.float32
        ).astype(jnp.bfloat16)
        return (key_rows, value_rows)

    projected = [source_heads(layer_index) for layer_index in range(layers)]
    every_key = jnp.stack([entry[0] for entry in projected])
    every_value = jnp.stack([entry[1] for entry in projected])
    every_key, every_value = (
        lax.all_gather(every_key, "sp", axis=1, tiled=True),
        lax.all_gather(every_value, "sp", axis=1, tiled=True),
    )
    sp_count = lax.axis_size("sp")
    source_rows = source.shape[0]
    grouping = 1
    while grouping * 2 * source_rows <= 512 and sp_count % (grouping * 2) == 0:
        grouping = grouping * 2
    stream = target
    for layer_index in range(layers):
        layer_gains = target_gains[layer_index]
        normed = rms_norm(stream, layer_gains[0]).astype(jnp.bfloat16)

        def query_piece(row_piece, offset, layer_index=layer_index):
            return jnp.dot(
                row_piece, query_weight[layer_index], preferred_element_type=jnp.float32
            ).astype(jnp.bfloat16)

        queries = query_piece(lax.all_gather(normed, "tp", axis=0, tiled=True), jnp.int32(0))
        group_rows = queries.shape[0]
        query_heads = queries.reshape(group_rows, heads_dev, HEAD_DIM)

        def attend(folded, pieces, offset, query_heads=query_heads):
            running_max, running_sum, weighted = folded
            key_heads = pieces[0].reshape(pieces[0].shape[0], heads_dev, HEAD_DIM)
            value_heads = pieces[1].reshape(pieces[1].shape[0], heads_dev, HEAD_DIM)
            scores = (
                jnp.einsum(
                    "thd,shd->ths", query_heads, key_heads, preferred_element_type=jnp.float32
                )
                * factor
            )
            new_max = jnp.maximum(running_max, jnp.max(scores, axis=-1))
            shrink = jnp.exp(running_max - new_max)
            weights = jnp.exp(scores - new_max[..., None])
            running_sum = running_sum * shrink + jnp.sum(weights, axis=-1)
            weighted = weighted * shrink[..., None] + jnp.einsum(
                "ths,shd->thd",
                weights.astype(jnp.bfloat16),
                value_heads,
                preferred_element_type=jnp.float32,
            )
            return (new_max, running_sum, weighted)

        initial = (
            jnp.full((group_rows, heads_dev), -1e30, jnp.float32),
            jnp.zeros((group_rows, heads_dev), jnp.float32),
            jnp.zeros((group_rows, heads_dev, HEAD_DIM), jnp.float32),
        )
        columns = every_key.shape[2]
        key_blocks = every_key[layer_index].reshape(
            sp_count // grouping, grouping * source_rows, columns
        )
        value_blocks = every_value[layer_index].reshape(
            sp_count // grouping, grouping * source_rows, columns
        )

        def scan_step(carry, blocks, attend=attend):
            return (attend(carry, blocks, 0), None)

        folded, unused = lax.scan(scan_step, initial, (key_blocks, value_blocks))
        running_max, running_sum, weighted = folded
        context = (
            (weighted / running_sum[..., None])
            .reshape(group_rows, heads_dev * HEAD_DIM)
            .astype(jnp.bfloat16)
        )

        def attn_term(offset, length, layer_index=layer_index, context=context):
            return jnp.dot(context, out_weight[layer_index], preferred_element_type=jnp.float32)

        attended = lax.psum_scatter(
            attn_term(jnp.int32(0), lax.axis_size("tp") * own_rows).astype(jnp.bfloat16),
            "tp",
            scatter_dimension=0,
            tiled=True,
        )
        stream = (stream.astype(jnp.float32) + rms_norm(attended, layer_gains[1])).astype(
            jnp.bfloat16
        )
        mixer_in = rms_norm(stream, layer_gains[2]).astype(jnp.bfloat16)

        def mixer_piece(row_piece, offset, layer_index=layer_index):
            gate_part = jnp.dot(
                row_piece, gate_weight[layer_index], preferred_element_type=jnp.float32
            )
            up_part = jnp.dot(row_piece, up_weight[layer_index], preferred_element_type=jnp.float32)
            return (jax.nn.silu(gate_part) * up_part).astype(jnp.bfloat16)

        hidden = mixer_piece(lax.all_gather(mixer_in, "tp", axis=0, tiled=True), jnp.int32(0))

        def mixer_term(offset, length, layer_index=layer_index, hidden=hidden):
            return jnp.dot(hidden, down_weight[layer_index], preferred_element_type=jnp.float32)

        mixer_out = lax.psum_scatter(
            mixer_term(jnp.int32(0), lax.axis_size("tp") * own_rows).astype(jnp.bfloat16),
            "tp",
            scatter_dimension=0,
            tiled=True,
        )
        stream = (stream.astype(jnp.float32) + rms_norm(mixer_out, layer_gains[3])).astype(
            jnp.bfloat16
        )
    return stream


def solution(mesh):
    placed = (
        P(("sp", "tp"), None),
        P("sp", None),
        P(),
        P(),
        P(None, None, "tp"),
        P(None, None, "tp"),
        P(None, None, "tp"),
        P(None, "tp", None),
        P(None, None, "tp"),
        P(None, None, "tp"),
        P(None, "tp", None),
    )
    return jax.shard_map(
        per_device, mesh=mesh, in_specs=placed, out_specs=P(("sp", "tp"), None), check_vma=False
    )
```

profile of v0, /device:TPU:0, one launch (start us, length us, event | category | flops | bytes accessed | tf_op | source)
XLA Modules:
  0.0 289.4 jit_solution(3847300409402123840)
XLA Ops:
  8.5 1.8 fusion.58
  10.3 1.6 fusion.59
  14.6 2.3 all_gather.19
  17.4 73.8 %all-gather.5.cloned.1.call-done = bf16[2,2048,512]{2,1,0:T(8,128)(2,1)} async-done(((bf16[2,128,512]{2,1,0:T(8,128)(2,1)}), bf16[2,2048,512]{2,1,0:T(8,128)(2,1)}) %all-gather.5.cloned.1.call-update) | async-done | bytes 4194320 | tf_op jit(solution)/shard_map/all_gather | solution.py:51
  91.3 4.5 %fusion.130 = (bf16[1,2048,512]{2,1,0:T(8,128)(2,1)}, bf16[1,2048,512]{2,1,0:T(8,128)(2,1)}) fusion(bf16[2,2048,512]{2,1,0:T(8,128)(2,1)} %all-gather.5.cloned.1.call-done), kind=kLoop, calls=%fused_computation.178 | loop fusion | bytes 8388608 | tf_op jit(solution)/shard_map/slice | solution.py:103
  95.7 72.7 %all-gather.3.cloned.1.call-done = bf16[2,2048,512]{2,1,0:T(8,128)(2,1)} async-done(((bf16[2,128,512]{2,1,0:T(8,128)(2,1)}), bf16[2,2048,512]{2,1,0:T(8,128)(2,1)}) %all-gather.3.cloned.1.call-update) | async-done | bytes 4194320 | tf_op jit(solution)/shard_map/all_gather | solution.py:50
  168.4 4.5 %fusion.131 = (bf16[1,2048,512]{2,1,0:T(8,128)(2,1)}, bf16[1,2048,512]{2,1,0:T(8,128)(2,1)}) fusion(bf16[2,2048,512]{2,1,0:T(8,128)(2,1)} %all-gather.3.cloned.1.call-done), kind=kLoop, calls=%fused_computation.179 | loop fusion | bytes 8388608 | tf_op jit(solution)/shard_map/slice | solution.py:100
  172.9 19.0 %while.30 = (s32[]{:T(128)}, f32[256,4]{0,1:T(4,128)S(1)}, f32[256,4]{0,1:T(4,128)S(1)}, f32[256,4,128]{0,2,1:T(8,128)}, bf16[4,512,512]{2,1,0:T(8,128)(2,1)}, /...) while((s32[]{:T(128)}, f32[256,4]{0,1:T(4,128)S(1)}, ...), condition=%wide.region_5.0_spmd.clone, body=%wide.region_2.5_spmd.clone.sunk | while | flops 273028096 | bytes 12910701 | solution.py:110
  175.5 1.4 fusion.166
  179.5 2.4 fusion.166
  184.5 2.4 fusion.166
  189.5 2.4 fusion.166
  193.1 2.5 convolution_convert_fusion.1
  195.6 6.6 %reduce-scatter.5.cloned.1.call-done = bf16[128,1024]{1,0:T(8,128)(2,1)} async-done(((bf16[256,1024]{1,0:T(8,128)(2,1)}), bf16[128,1024]{1,0:T(8,128)(2,1)}) %reduce-scatter.5.cloned.1.call-update) | async-done | bytes 262160 | tf_op jit(solution)/shard_map/reduce_scatter | solution.py:121
  204.7 2.2 all_gather.21
  206.9 2.0 fusion.28
  208.9 4.0 %fusion.39 = bf16[256,1024]{1,0:T(8,128)(2,1)} fusion(bf16[2,768,1024]{2,1,0:T(8,128)(2,1)} %param.25, bf16[256,1024]{1,0:T(8,128)(2,1)S(1)} %all_gather.21, bf16[2,1024,768]{2,1,0:T(8,128)(2,1)} %param.24, f32[256,768]{1,0:T(8,128)S(1)} %fusion.28), kind=kOutput, calls=%fused_computation.55 | convolution fusion | flops 806748160 | bytes 4980736 | tf_op jit(solution)/shard_map/dot_general | solution.py:142
  213.0 9.1 %reduce-scatter.7.cloned.1.call-done = bf16[128,1024]{1,0:T(8,128)(2,1)} async-done(((bf16[256,1024]{1,0:T(8,128)(2,1)}), bf16[128,1024]{1,0:T(8,128)(2,1)}) %reduce-scatter.7.cloned.1.call-update) | async-done | bytes 262160 | tf_op jit(solution)/shard_map/reduce_scatter | solution.py:144
  225.3 2.2 all_gather.22
  228.0 19.0 %while.31 = (s32[]{:T(128)}, f32[256,4]{0,1:T(4,128)S(1)}, f32[256,4]{0,1:T(4,128)S(1)}, f32[256,4,128]{0,2,1:T(8,128)}, bf16[4,512,512]{2,1,0:T(8,128)(2,1)}, /...) while((s32[]{:T(128)}, f32[256,4]{0,1:T(4,128)S(1)}, ...), condition=%wide.region_15.16_spmd.clone, body=%wide.region_12.0_spmd.clone.sunk | while | flops 273028096 | bytes 12910701 | solution.py:110
  228.0 1.3 constant_dynamic-slice_fusion.7
  230.6 1.4 fusion.173
  234.6 2.4 fusion.173
  239.6 2.4 fusion.173
  244.6 2.4 fusion.173
  248.1 2.5 convolution_convert_fusion
  250.7 9.1 %reduce-scatter.9.cloned.1.call-done = bf16[128,1024]{1,0:T(8,128)(2,1)} async-done(((bf16[256,1024]{1,0:T(8,128)(2,1)}), bf16[128,1024]{1,0:T(8,128)(2,1)}) %reduce-scatter.9.cloned.1.call-update) | async-done | bytes 262160 | tf_op jit(solution)/shard_map/reduce_scatter | solution.py:121
  262.3 2.2 all_gather.23
  264.5 2.0 fusion.22
  266.5 4.0 %fusion.45 = bf16[256,1024]{1,0:T(8,128)(2,1)} fusion(bf16[2,768,1024]{2,1,0:T(8,128)(2,1)} %param.25, bf16[256,1024]{1,0:T(8,128)(2,1)S(1)} %all_gather.23, bf16[2,1024,768]{2,1,0:T(8,128)(2,1)} %param.24, f32[256,768]{1,0:T(8,128)S(1)} %fusion.22), kind=kOutput, calls=%fused_computation.57 | convolution fusion | flops 806748160 | bytes 4980736 | tf_op jit(solution)/shard_map/dot_general | solution.py:142
  270.5 9.2 %reduce-scatter.11.cloned.1.call-done = bf16[128,1024]{1,0:T(8,128)(2,1)} async-done(((bf16[256,1024]{1,0:T(8,128)(2,1)}), bf16[128,1024]{1,0:T(8,128)(2,1)}) %reduce-scatter.11.cloned.1.call-update) | async-done | bytes 262160 | tf_op jit(solution)/shard_map/reduce_scatter | solution.py:144
  280.7 1.8 fusion.118
  (133 shorter events, 36.6 us)
Async XLA Ops:
  6.5 3.8 %copy-start.4 = (bf16[128,1024]{1,0:T(8,128)(2,1)S(1)}, bf16[128,1024]{1,0:T(8,128)(2,1)}, u32[]{:S(2)}) copy-start(bf16[128,1024]{1,0:T(8,128)(2,1)} %param.16) | copy-start | bytes 786436
  6.5 84.7 %all-gather.5.cloned.1.call-start = ((), (), s32[]{:S(2)}) async-start(), calls=%async_computation.5 | async-start | bytes 4456448 | tf_op jit(solution)/shard_map/all_gather | solution.py:51
  8.5 4.3 %copy-start.6 = (bf16[2,1024,512]{2,1,0:T(8,128)(2,1)S(1)}, bf16[2,1024,512]{2,1,0:T(8,128)(2,1)}, u32[]{:S(2)}) copy-start(bf16[2,1024,512]{2,1,0:T(8,128)(2,1)} %param.20) | copy-start | bytes 6291460
  12.7 1.7 copy-start
  12.7 1.8 copy-start.5
  12.7 155.7 %all-gather.3.cloned.1.call-start = ((), (), s32[]{:S(2)}) async-start(), calls=%async_computation.4 | async-start | bytes 4456448 | tf_op jit(solution)/shard_map/all_gather | solution.py:50
  13.5 3.5 %copy-start.7 = (bf16[2,1024,512]{2,1,0:T(8,128)(2,1)S(1)}, bf16[2,1024,512]{2,1,0:T(8,128)(2,1)}, u32[]{:S(2)}) copy-start(bf16[2,1024,512]{2,1,0:T(8,128)(2,1)} %param.19) | copy-start | bytes 6291460
  14.2 188.0 %reduce-scatter.5.cloned.1.call-start = ((), (), s32[]{:S(2)}) async-start(), calls=%async_computation.6 | async-start | bytes 786432 | tf_op jit(solution)/shard_map/reduce_scatter | solution.py:121
  191.9 11.4 %copy-start.1 = (bf16[128,1024]{1,0:T(8,128)(2,1)S(1)}, bf16[128,1024]{1,0:T(8,128)(2,1)}, u32[]{:S(2)}) copy-start(bf16[128,1024]{1,0:T(8,128)(2,1)} %param.15) | copy-start | bytes 786436
  195.6 26.5 %reduce-scatter.7.cloned.1.call-start = ((), (), s32[]{:S(2)}) async-start(), calls=%async_computation.7 | async-start | bytes 786432 | tf_op jit(solution)/shard_map/reduce_scatter | solution.py:144
  212.9 14.6 %copy-start.8 = (bf16[2,1024,512]{2,1,0:T(8,128)(2,1)S(1)}, bf16[2,1024,512]{2,1,0:T(8,128)(2,1)}, u32[]{:S(2)}) copy-start(bf16[2,1024,512]{2,1,0:T(8,128)(2,1)} %param.19) | copy-start | bytes 6291460
  212.9 46.9 %reduce-scatter.9.cloned.1.call-start = ((), (), s32[]{:S(2)}) async-start(), calls=%async_computation.8 | async-start | bytes 786432 | tf_op jit(solution)/shard_map/reduce_scatter | solution.py:121
  224.4 0.7 copy-start.2
  247.0 13.9 %copy-start.3 = (bf16[128,1024]{1,0:T(8,128)(2,1)S(1)}, bf16[128,1024]{1,0:T(8,128)(2,1)}, u32[]{:S(2)}) copy-start(bf16[128,1024]{1,0:T(8,128)(2,1)} %copy-done.2) | copy-start | bytes 786436
  250.6 29.0 %reduce-scatter.11.cloned.1.call-start = ((), (), s32[]{:S(2)}) async-start(), calls=%async_computation.9 | async-start | bytes 786432 | tf_op jit(solution)/shard_map/reduce_scatter | solution.py:144
Sparse Core Ops, SparseCore 0:
  12.8 78.4 all-gather.4
  94.0 74.3 all-gather.2
  195.7 6.4 reduce-scatter.4
  213.0 9.0 reduce-scatter.6
  250.7 9.0 reduce-scatter.8
  270.6 9.0 reduce-scatter.10
where the time goes:
time: 291 us; the launch traced here: 289 us
  waiting for transfers between devices  181 us (62%)
  matrix products  43 us (15%)
  local copies, waits for them, and re-layouts  23.3 us (8%)
  other arithmetic  19.4 us (7%)
  between operations  13.7 us (5%)
  blocking collectives  8.84 us (3%)
    all_gather x1, waiting for transfers between devices, per_device(): lax.all_gather(every_value, 'sp', axis=1, tiled=True)  73.8 us
    all_gather x1, waiting for transfers between devices, per_device(): lax.all_gather(every_key, 'sp', axis=1, tiled=True)  72.7 us
    reduce_scatter x2, waiting for transfers between devices, per_device(): lax.psum_scatter(mixer_term(jnp.int32(0), lax.axis_size('tp') * own_rows)...  18.3 us
    dot_general x8, matrix products, attend(): jnp.einsum('ths,shd->thd', weights.astype(jnp.bfloat16), value_heads, pre...  17.1 us
    reduce_scatter x2, waiting for transfers between devices, per_device(): lax.psum_scatter(attn_term(jnp.int32(0), lax.axis_size('tp') * own_rows)....  15.8 us
    dynamic_slice x24, local copies, waits for them, and re-layouts, per_device(): folded, unused = lax.scan(scan_step, initial, (key_blocks, value_blocks))  13.5 us
    reduce_sum x9, other arithmetic, rms_norm(): jnp.mean(widened * widened, axis=-1, keepdims=True) + epsilon  9.31 us
    dot_general x2, matrix products, mixer_term(): jnp.dot(hidden, down_weight[layer_index], preferred_element_type=jnp.floa...  7.98 us
  transfers between devices with their start and end apart: 6, of which 6 were waited for; matrix products, arithmetic and copies ran while one was open for 2% of the time, Pallas kernels for 0%

commit v1 on v0

--- a/solution.py
+++ b/solution.py
@@ -1,6 +1,11 @@
+import functools
+import math
+
 import jax
 import jax.numpy as jnp
 from jax import lax
+from jax.experimental import pallas as pl
+from jax.experimental.pallas import tpu as pltpu
 from jax.sharding import PartitionSpec as P
 
 HEAD_DIM = 128
@@ -153,6 +158,400 @@
     return stream
 
 
+MESH = pl.DeviceIdType.MESH
+F32 = jnp.float32
+BF16 = jnp.bfloat16
+KZ, KX, KY, KDX, KDY, TZ, TX, TY, TDX, TDY = range(10)
+
+
+def dot(a, b):
+    return jnp.dot(a, b, preferred_element_type=F32)
+
+
+def fused_kernel(
+    grid,
+    target,
+    source,
+    target_gains,
+    source_gain,
+    wq_hbm,
+    wk_hbm,
+    wv_hbm,
+    wo_hbm,
+    wg_hbm,
+    wu_hbm,
+    wd_hbm,
+    out_ref,
+    stream,
+    src,
+    wq,
+    wk,
+    wv,
+    wo,
+    wg,
+    wu,
+    wd,
+    keys,
+    values,
+    queries,
+    maxima,
+    acc,
+    part,
+    got,
+    send,
+    recv,
+    xsend,
+    xrecv,
+    wsem,
+    lsem,
+):
+    size_x, size_y, size_z = grid
+    layers = wq.shape[0]
+    own = target.shape[0]
+    rows = source.shape[0]
+    heads = wq.shape[2] // HEAD_DIM
+    half, quarter = rows // 2, rows // 4
+    chunk = 4 * rows
+    sp = lax.axis_index("sp")
+    core = lax.axis_index("tp")
+    other = 1 - core
+    x = lax.rem(sp, size_x)
+    y = lax.rem(lax.div(sp, size_x), size_y)
+    z = lax.div(sp, size_x * size_y)
+
+    def at(xx, yy, zz, cc):
+        return {"sp": (zz * size_y + yy) * size_x + xx, "tp": cc}
+
+    def flip(j):
+        low = lax.rem(lax.rem(z, 2) + j % 2, 2)
+        high = lax.rem(lax.div(z, 2) + j // 2, 2)
+        return low + 2 * high
+
+    x_peer = at(1 - x, y, z, core)
+    y_peer = at(x, 1 - y, z, core)
+    tp_peer = at(x, y, z, other)
+    z_peers = [at(x, y, flip(j), core) for j in range(size_z)]
+
+    own_rows = pl.ds(pl.multiple_of(core * own, own), own)
+    other_rows = pl.ds(pl.multiple_of(other * own, own), own)
+    source_copy = pltpu.make_async_copy(source, src.at[0, 0], lsem.at[0])
+    target_copy = pltpu.make_async_copy(target, stream.at[own_rows], lsem.at[1])
+    source_copy.start()
+    target_copy.start()
+    pairs = [(wk_hbm, wk), (wv_hbm, wv), (wq_hbm, wq), (wo_hbm, wo), (wg_hbm, wg), (wu_hbm, wu), (wd_hbm, wd)]
+    fetch = {}
+    for layer in range(layers):
+        for k, (a, b) in enumerate(pairs):
+            fetch[k, layer] = pltpu.make_async_copy(a.at[layer], b.at[layer], wsem.at[k, layer])
+
+    barrier = pltpu.get_barrier_semaphore()
+    peers = [x_peer, y_peer, tp_peer] + z_peers[1:]
+    for peer in peers:
+        pl.semaphore_signal(barrier, inc=1, device_id=peer, device_id_type=MESH)
+    for k in (2, 0, 1):
+        fetch[k, 0].start()
+    for k in (0, 1):
+        for layer in range(1, layers):
+            fetch[k, layer].start()
+    pl.semaphore_wait(barrier, len(peers))
+
+    def mine(c):
+        return pl.ds(pl.multiple_of(c * half, half), half)
+
+    def first(c):
+        return pl.ds(pl.multiple_of(c * half, quarter), quarter)
+
+    def second(c):
+        return pl.ds(pl.multiple_of(c * half + quarter, quarter), quarter)
+
+    def copy(kind, j, from_ref, to_ref, peer):
+        return pltpu.make_async_remote_copy(
+            src_ref=from_ref,
+            dst_ref=to_ref,
+            send_sem=send.at[kind, j],
+            recv_sem=recv.at[kind, j],
+            device_id=peer,
+            device_id_type=MESH,
+        )
+
+    def blk(j, sub, sl):
+        return src.at[j, sub, sl]
+
+    def to_z(j):
+        return copy(KZ, j, blk(0, 0, mine(core)), blk(j, 0, mine(core)), z_peers[j])
+
+    def to_x(j):
+        return copy(KX, j, blk(j, 0, mine(core)), blk(j, 1, mine(core)), x_peer)
+
+    def to_y(j):
+        return copy(KY, j, blk(j, 0, mine(core)), blk(j, 2, mine(core)), y_peer)
+
+    def diag_y(j):
+        return copy(KDY, j, blk(j, 1, first(core)), blk(j, 3, first(core)), y_peer)
+
+    def diag_x(j):
+        return copy(KDX, j, blk(j, 2, second(core)), blk(j, 3, second(core)), x_peer)
+
+    def to_tp(kind, j, c):
+        sub = {TZ: 0, TX: 1, TY: 2, TDX: 3, TDY: 3}[kind]
+        sl = {TDX: second, TDY: first}.get(kind, mine)(c)
+        return copy(kind, j, blk(j, sub, sl), blk(j, sub, sl), tp_peer)
+
+    def z_arrived(zj, static):
+        copy(KZ, zj, blk(zj, 0, mine(core)), blk(zj, 0, mine(core)), x_peer).wait_recv()
+        to_x(zj).start()
+        to_y(zj).start()
+        to_tp(TZ, zj, core).start()
+
+    def xy_arrived(j):
+        copy(KX, j, blk(j, 1, mine(core)), blk(j, 1, mine(core)), x_peer).wait_recv()
+        diag_y(j).start()
+        to_tp(TX, j, core).start()
+        copy(KY, j, blk(j, 2, mine(core)), blk(j, 2, mine(core)), y_peer).wait_recv()
+        diag_x(j).start()
+        to_tp(TY, j, core).start()
+
+    def diag_arrived(j):
+        copy(KDY, j, blk(j, 3, first(core)), blk(j, 3, first(core)), y_peer).wait_recv()
+        to_tp(TDY, j, core).start()
+        copy(KDX, j, blk(j, 3, second(core)), blk(j, 3, second(core)), x_peer).wait_recv()
+        to_tp(TDX, j, core).start()
+
+    def xcopy(e, from_ref, to_ref):
+        return pltpu.make_async_remote_copy(
+            src_ref=from_ref,
+            dst_ref=to_ref,
+            send_sem=xsend.at[e],
+            recv_sem=xrecv.at[e],
+            device_id=tp_peer,
+            device_id_type=MESH,
+        )
+
+    source_copy.wait()
+    to_x(0).start()
+    to_y(0).start()
+    for j in range(1, size_z):
+        to_z(j).start()
+    target_copy.wait()
+    give = xcopy(0, stream.at[own_rows], stream.at[own_rows])
+    give.start()
+    for layer in range(layers):
+        for k in (2, 3, 4, 5, 6):
+            if (k, layer) != (2, 0):
+                fetch[k, layer].start()
+
+    def rms(v, gain):
+        inverse = lax.rsqrt(jnp.mean(v * v, axis=-1, keepdims=True) + epsilon)
+        return v * inverse * gain.astype(F32)
+
+    scale = HEAD_DIM ** (-0.5) * math.log2(math.e)
+
+    def project_queries(layer):
+        normed = rms(stream[...].astype(F32), target_gains[layer, 0:1]).astype(BF16)
+        queries[...] = (dot(normed, wq[layer]) * scale).astype(BF16)
+        maxima[...] = jnp.full(maxima.shape, -1e30, F32)
+        acc[...] = jnp.zeros(acc.shape, F32)
+
+    def project_source(layer, j):
+        normed = rms(
+            src[j].reshape(chunk, src.shape[-1]).astype(F32), source_gain[layer : layer + 1]
+        ).astype(BF16)
+        keys[layer, j] = dot(normed, wk[layer]).astype(BF16)
+        values[layer, j] = dot(normed, wv[layer]).astype(BF16)
+
+    def attend(layer, j):
+        for h in range(heads):
+            cols = slice(h * HEAD_DIM, (h + 1) * HEAD_DIM)
+            scores = lax.dot_general(
+                queries[:, cols],
+                keys[layer, j, :, cols],
+                (((1,), (1,)), ((), ())),
+                preferred_element_type=F32,
+            )
+            old = maxima[h]
+            new = jnp.maximum(old, jnp.max(scores, axis=-1, keepdims=True))
+            maxima[h] = new
+            shrink = jnp.exp2(old - new)
+            weights = jnp.exp2(scores - jnp.concatenate([new] * (chunk // HEAD_DIM), axis=1))
+            block = values[layer, j, :, cols]
+            block = jnp.concatenate([block, jnp.ones(block.shape, BF16)], axis=1)
+            acc[h] = acc[h] * jnp.concatenate([shrink, shrink], axis=1) + dot(
+                weights.astype(BF16), block
+            )
+
+    z_arrived(1, True)
+    xcopy(0, stream.at[other_rows], stream.at[other_rows]).wait_recv()
+    fetch[2, 0].wait()
+    project_queries(0)
+    xy_arrived(0)
+    for k in (0, 1):
+        for layer in range(layers):
+            fetch[k, layer].wait()
+
+    def plane(j, unused):
+        @pl.when(j + 2 < size_z)
+        def _():
+            z_arrived(j + 2, False)
+
+        @pl.when(j + 1 < size_z)
+        def _():
+            xy_arrived(j + 1)
+
+        diag_arrived(j)
+
+        @pl.when(j > 0)
+        def _():
+            to_tp(TZ, j, other).wait_recv()
+
+        for kind in (TX, TY, TDX, TDY):
+            to_tp(kind, j, other).wait_recv()
+        for layer in range(layers):
+            project_source(layer, j)
+        attend(0, j)
+        return unused
+
+    lax.fori_loop(0, size_z, plane, 0)
+
+    def exchanged(e, rows_of):
+        return (
+            part[e, rows_of].astype(F32) + got[e, rows_of].astype(F32)
+        ).astype(BF16).astype(F32)
+
+    give.wait_send()
+    pending = []
+    exchange = 0
+    for layer in range(layers):
+        if layer > 0:
+            fetch[2, layer].wait()
+            project_queries(layer)
+
+            def again(j, unused, layer=layer):
+                attend(layer, j)
+                return unused
+
+            lax.fori_loop(0, size_z, again, 0)
+        fetch[3, layer].wait()
+        e = exchange
+        exchange += 1
+        copies = []
+        for b in range(2):
+            sl = slice(b * own, (b + 1) * own)
+            context = jnp.concatenate(
+                [
+                    (acc[h, sl, :HEAD_DIM] / acc[h, sl, HEAD_DIM:]).astype(BF16)
+                    for h in range(heads)
+                ],
+                axis=1,
+            )
+            part[e, sl] = dot(context, wo[layer]).astype(BF16)
+            c = xcopy(1 + 2 * e + b, part.at[e, sl], got.at[e, sl])
+            c.start()
+            copies.append(c)
+        for k in (4, 5, 6):
+            fetch[k, layer].wait()
+        for b in range(2):
+            sl = slice(b * own, (b + 1) * own)
+            copies[b].wait_recv()
+            stream[sl] = (
+                stream[sl].astype(F32) + rms(exchanged(e, sl), target_gains[layer, 1:2])
+            ).astype(BF16)
+        pending += copies
+        mixer_in = rms(stream[...].astype(F32), target_gains[layer, 2:3]).astype(BF16)
+        gate = dot(mixer_in, wg[layer])
+        hidden = (gate / (1.0 + jnp.exp(-gate)) * dot(mixer_in, wu[layer])).astype(BF16)
+        e = exchange
+        exchange += 1
+        part[e] = dot(hidden, wd[layer]).astype(BF16)
+        if layer < layers - 1:
+            copies = []
+            for b in range(2):
+                sl = slice(b * own, (b + 1) * own)
+                c = xcopy(1 + 2 * e + b, part.at[e, sl], got.at[e, sl])
+                c.start()
+                copies.append(c)
+            for b in range(2):
+                sl = slice(b * own, (b + 1) * own)
+                copies[b].wait_recv()
+                stream[sl] = (
+                    stream[sl].astype(F32) + rms(exchanged(e, sl), target_gains[layer, 3:4])
+                ).astype(BF16)
+            pending += copies
+        else:
+            c = xcopy(1 + 2 * e, part.at[e, other_rows], got.at[e, other_rows])
+            c.start()
+            xcopy(1 + 2 * e, part.at[e, own_rows], got.at[e, own_rows]).wait_recv()
+            out_ref[...] = (
+                stream[own_rows].astype(F32)
+                + rms(exchanged(e, own_rows), target_gains[layer, 3:4])
+            ).astype(BF16)
+            pending.append(c)
+    for c in pending:
+        c.wait_send()
+    for j in range(size_z):
+        if j > 0:
+            to_z(j).wait_send()
+            to_tp(TZ, j, core).wait_send()
+        to_x(j).wait_send()
+        to_y(j).wait_send()
+        diag_x(j).wait_send()
+        diag_y(j).wait_send()
+        for kind in (TX, TY, TDX, TDY):
+            to_tp(kind, j, core).wait_send()
+
+
+def fused(grid, *args):
+    target, source, target_gains, source_gain, wq, wk, wv, wo, wg, wu, wd = args
+    layers, width, columns = wq.shape
+    own, rows = target.shape[0], source.shape[0]
+    heads = columns // HEAD_DIM
+    size_z = grid[2]
+    any_spec = pl.BlockSpec(memory_space=pl.ANY)
+    vmem_spec = pl.BlockSpec(memory_space=pltpu.VMEM)
+    return pl.pallas_call(
+        functools.partial(fused_kernel, grid),
+        out_shape=jax.ShapeDtypeStruct(target.shape, BF16),
+        in_specs=[any_spec, any_spec, vmem_spec, vmem_spec] + [any_spec] * 7,
+        out_specs=vmem_spec,
+        scratch_shapes=[
+            pltpu.VMEM((2 * own, width), BF16),
+            pltpu.VMEM((size_z, 4, rows, width), BF16),
+            *[pltpu.VMEM(w.shape, BF16) for w in (wq, wk, wv, wo, wg, wu, wd)],
+            pltpu.VMEM((layers, size_z, 4 * rows, columns), BF16),
+            pltpu.VMEM((layers, size_z, 4 * rows, columns), BF16),
+            pltpu.VMEM((2 * own, columns), BF16),
+            pltpu.VMEM((heads, 2 * own, HEAD_DIM), F32),
+            pltpu.VMEM((heads, 2 * own, 2 * HEAD_DIM), F32),
+            pltpu.VMEM((2 * layers, 2 * own, width), BF16),
+            pltpu.VMEM((2 * layers, 2 * own, width), BF16),
+            pltpu.SemaphoreType.DMA((10, size_z)),
+            pltpu.SemaphoreType.DMA((10, size_z)),
+            pltpu.SemaphoreType.DMA((1 + 4 * layers,)),
+            pltpu.SemaphoreType.DMA((1 + 4 * layers,)),
+            pltpu.SemaphoreType.DMA((7, layers)),
+            pltpu.SemaphoreType.DMA((2,)),
+        ],
+        compiler_params=pltpu.CompilerParams(
+            collective_id=0, has_side_effects=True, vmem_limit_bytes=60 * 1024 * 1024
+        ),
+    )(*args)
+
+
+def chip_grid(mesh):
+    devices = mesh.devices
+    if mesh.axis_names != ("sp", "tp") or devices.shape[1] != 2:
+        return None
+    places = [tuple(d.coords) for d in devices[:, 0]]
+    if [tuple(d.coords) for d in devices[:, 1]] != places:
+        return None
+    grid = tuple(max(p[k] for p in places) + 1 for k in range(3))
+    expected = [
+        (x, y, z) for z in range(grid[2]) for y in range(grid[1]) for x in range(grid[0])
+    ]
+    if places != expected or grid != (2, 2, 4):
+        return None
+    return grid
+
+
 def solution(mesh):
     placed = (
         P(("sp", "tp"), None),
@@ -167,6 +566,8 @@
         P(None, None, "tp"),
         P(None, "tp", None),
     )
+    grid = chip_grid(mesh)
+    body = per_device if grid is None else functools.partial(fused, grid)
     return jax.shard_map(
-        per_device, mesh=mesh, in_specs=placed, out_specs=P(("sp", "tp"), None), check_vma=False
+        body, mesh=mesh, in_specs=placed, out_specs=P(("sp", "tp"), None), check_vma=False
     )

time: 291 us -> 57.5 us (0.20)
  waiting for transfers between devices: 181 us -> 0 us
  Pallas kernels: 0 us -> 55.6 us
  matrix products: 43 us -> 0 us
  local copies, waits for them, and re-layouts: 23.3 us -> 1.67 us
  other arithmetic: 19.4 us -> 0 us
  between operations: 13.7 us -> 0.01 us
  blocking collectives: 8.84 us -> 0 us
    all_gather x2 -> x0, waiting for transfers between devices: 146 us -> none  [the longest x1 73.8 us: per_device(): lax.all_gather(every_value, 'sp', axis=1, tiled=True)]
    pallas_call x0 -> x1, Pallas kernels: none -> 55.6 us  [fused(): pl.pallas_call(functools.partial(fused_kernel, grid), out_shape=jax.Shape...]
    dot_general x28 -> x0, matrix products: 43 us -> none  [the longest x8 17.1 us: attend(): jnp.einsum('ths,shd->thd', weights.astype(jnp.bfloat16), value_heads, pre...]
    reduce_scatter x4 -> x0, waiting for transfers between devices: 34.1 us -> none  [the longest x2 18.3 us: per_device(): lax.psum_scatter(mixer_term(jnp.int32(0), lax.axis_size('tp') * own_rows)...]
    dynamic_slice x24 -> x0, local copies, waits for them, and re-layouts: 13.5 us -> none  [per_device(): folded, unused = lax.scan(scan_step, initial, (key_blocks, value_blocks))]
    reduce_sum x17 -> x0, other arithmetic: 12.2 us -> none  [the longest x9 9.31 us: rms_norm(): jnp.mean(widened * widened, axis=-1, keepdims=True) + epsilon]
    slice x2 -> x0, local copies, waits for them, and re-layouts: 8.95 us -> none  [the longest x1 4.48 us: per_device(): every_key[layer_index]]
    all_gather x4 -> x0, blocking collectives: 8.84 us -> none  [the longest x2 4.48 us: per_device(): lax.all_gather(normed, 'tp', axis=0, tiled=True)]
  transfers between devices with their start and end apart: 6 -> 0, of which waited for: 6 -> 0; matrix products, arithmetic and copies ran while one was open for 2% -> 0% of each run, Pallas kernels for 0% -> 0%
where the time goes in v1:
time: 57.5 us; the launch traced here: 57.3 us
  Pallas kernels  55.6 us (97%)
  local copies, waits for them, and re-layouts  1.67 us (3%)
    pallas_call x1, Pallas kernels, fused(): pl.pallas_call(functools.partial(fused_kernel, grid), out_shape=jax.Shape...  55.6 us
    unnamed x1, local copies, waits for them, and re-layouts  1.67 us

profile of v1, /device:TPU:0, one launch (start us, length us, event | category | flops | bytes accessed | tf_op | source)
XLA Modules:
  0.0 57.3 jit_solution(16441999591078853918)
XLA Ops:
  0.0 55.6 %shard_map.109 = bf16[128,1024]{1,0:T(8,128)(2,1)} custom-call(bf16[128,1024]{1,0:T(8,128)(2,1)} %target.1, bf16[128,1024]{1,0:T(8,128)(2,1)} %source.1, bf16[2,4,1024]{2,1,0:T(4,128)(2,1)} %target_gains.1, bf16[2,1024]{1,0:T(2,128)(2,1)} %source_gain.1, bf16[2,1024,512]{2,1,0:T(8,128)(2,1)} %wq_hbm.1, bf16[2,1024,512]{2,1,0:T(8,128)(2,1)} %wk_hbm.1, ...), custom_call_target="tpu_custom_call" | custom-call | tf_op jit(solution)/shard_map/pallas_call | solution.py:510
  55.6 1.7 %copy.13 = bf16[128,1024]{1,0:T(8,128)(2,1)} copy(bf16[128,1024]{1,0:T(8,128)(2,1)} %shard_map.109) | data formatting | bytes 524288

commit v2 on v1

--- a/solution.py
+++ b/solution.py
@@ -223,14 +223,15 @@
         return {"sp": (zz * size_y + yy) * size_x + xx, "tp": cc}
 
     def flip(j):
-        low = lax.rem(lax.rem(z, 2) + j % 2, 2)
-        high = lax.rem(lax.div(z, 2) + j // 2, 2)
+        low = lax.rem(z + j, 2)
+        high = lax.rem(lax.div(z, 2) + lax.div(j, 2), 2)
         return low + 2 * high
 
     x_peer = at(1 - x, y, z, core)
     y_peer = at(x, 1 - y, z, core)
     tp_peer = at(x, y, z, other)
-    z_peers = [at(x, y, flip(j), core) for j in range(size_z)]
+    inner = lax.rem(lax.rem(z, 2) + lax.div(z, 2), 2)
+    order = [jnp.int32(0), jnp.int32(1), 2 + inner, 3 - inner]
 
     own_rows = pl.ds(pl.multiple_of(core * own, own), own)
     other_rows = pl.ds(pl.multiple_of(other * own, own), own)
@@ -245,7 +246,7 @@
             fetch[k, layer] = pltpu.make_async_copy(a.at[layer], b.at[layer], wsem.at[k, layer])
 
     barrier = pltpu.get_barrier_semaphore()
-    peers = [x_peer, y_peer, tp_peer] + z_peers[1:]
+    peers = [x_peer, y_peer, tp_peer] + [at(x, y, flip(j), core) for j in order[1:]]
     for peer in peers:
         pl.semaphore_signal(barrier, inc=1, device_id=peer, device_id_type=MESH)
     for k in (2, 0, 1):
@@ -278,7 +279,7 @@
         return src.at[j, sub, sl]
 
     def to_z(j):
-        return copy(KZ, j, blk(0, 0, mine(core)), blk(j, 0, mine(core)), z_peers[j])
+        return copy(KZ, j, blk(0, 0, mine(core)), blk(j, 0, mine(core)), at(x, y, flip(j), core))
 
     def to_x(j):
         return copy(KX, j, blk(j, 0, mine(core)), blk(j, 1, mine(core)), x_peer)
@@ -297,7 +298,7 @@
         sl = {TDX: second, TDY: first}.get(kind, mine)(c)
         return copy(kind, j, blk(j, sub, sl), blk(j, sub, sl), tp_peer)
 
-    def z_arrived(zj, static):
+    def z_arrived(zj):
         copy(KZ, zj, blk(zj, 0, mine(core)), blk(zj, 0, mine(core)), x_peer).wait_recv()
         to_x(zj).start()
         to_y(zj).start()
@@ -330,7 +331,7 @@
     source_copy.wait()
     to_x(0).start()
     to_y(0).start()
-    for j in range(1, size_z):
+    for j in order[1:]:
         to_z(j).start()
     target_copy.wait()
     give = xcopy(0, stream.at[own_rows], stream.at[own_rows])
@@ -379,45 +380,56 @@
                 weights.astype(BF16), block
             )
 
-    z_arrived(1, True)
+    def complete(j, step):
+        if step > 0:
+            to_tp(TZ, j, other).wait_recv()
+        for kind in (TX, TY, TDX, TDY):
+            to_tp(kind, j, other).wait_recv()
+
+    z_arrived(order[1])
     xcopy(0, stream.at[other_rows], stream.at[other_rows]).wait_recv()
     fetch[2, 0].wait()
     project_queries(0)
-    xy_arrived(0)
+    xy_arrived(order[0])
     for k in (0, 1):
         for layer in range(layers):
             fetch[k, layer].wait()
-
-    def plane(j, unused):
-        @pl.when(j + 2 < size_z)
-        def _():
-            z_arrived(j + 2, False)
-
-        @pl.when(j + 1 < size_z)
-        def _():
-            xy_arrived(j + 1)
-
-        diag_arrived(j)
-
-        @pl.when(j > 0)
-        def _():
-            to_tp(TZ, j, other).wait_recv()
-
-        for kind in (TX, TY, TDX, TDY):
-            to_tp(kind, j, other).wait_recv()
-        for layer in range(layers):
-            project_source(layer, j)
-        attend(0, j)
-        return unused
-
-    lax.fori_loop(0, size_z, plane, 0)
+    late = range(1, layers)
+    xy_arrived(order[1])
+    diag_arrived(order[0])
+    complete(order[0], 0)
+    project_source(0, order[0])
+    z_arrived(order[2])
+    for layer in late:
+        project_source(layer, order[0])
+    attend(0, order[0])
+    z_arrived(order[3])
+    diag_arrived(order[1])
+    complete(order[1], 1)
+    project_source(0, order[1])
+    xy_arrived(order[2])
+    for layer in late:
+        project_source(layer, order[1])
+    attend(0, order[1])
+    xy_arrived(order[3])
+    diag_arrived(order[2])
+    complete(order[2], 2)
+    project_source(0, order[2])
+    for layer in late:
+        project_source(layer, order[2])
+    diag_arrived(order[3])
+    attend(0, order[2])
+    complete(order[3], 3)
+    project_source(0, order[3])
+    attend(0, order[3])
+
+    give.wait_send()
 
     def exchanged(e, rows_of):
         return (
             part[e, rows_of].astype(F32) + got[e, rows_of].astype(F32)
         ).astype(BF16).astype(F32)
 
-    give.wait_send()
     pending = []
     exchange = 0
     for layer in range(layers):
@@ -449,6 +461,9 @@
             copies.append(c)
         for k in (4, 5, 6):
             fetch[k, layer].wait()
+        if layer == 0:
+            for k in late:
+                project_source(k, order[3])
         for b in range(2):
             sl = slice(b * own, (b + 1) * own)
             copies[b].wait_recv()
@@ -461,11 +476,11 @@
         hidden = (gate / (1.0 + jnp.exp(-gate)) * dot(mixer_in, wu[layer])).astype(BF16)
         e = exchange
         exchange += 1
-        part[e] = dot(hidden, wd[layer]).astype(BF16)
         if layer < layers - 1:
             copies = []
             for b in range(2):
                 sl = slice(b * own, (b + 1) * own)
+                part[e, sl] = dot(hidden[sl], wd[layer]).astype(BF16)
                 c = xcopy(1 + 2 * e + b, part.at[e, sl], got.at[e, sl])
                 c.start()
                 copies.append(c)
@@ -477,6 +492,7 @@
                 ).astype(BF16)
             pending += copies
         else:
+            part[e] = dot(hidden, wd[layer]).astype(BF16)
             c = xcopy(1 + 2 * e, part.at[e, other_rows], got.at[e, other_rows])
             c.start()
             xcopy(1 + 2 * e, part.at[e, own_rows], got.at[e, own_rows]).wait_recv()
@@ -487,8 +503,8 @@
             pending.append(c)
     for c in pending:
         c.wait_send()
-    for j in range(size_z):
-        if j > 0:
+    for step, j in enumerate(order):
+        if step > 0:
             to_z(j).wait_send()
             to_tp(TZ, j, core).wait_send()
         to_x(j).wait_send()

time: 57.5 us -> 54.5 us (0.948)
  Pallas kernels: 55.6 us -> 52.6 us
    pallas_call x1, Pallas kernels: 55.6 us -> 52.6 us  [fused(): pl.pallas_call(functools.partial(fused_kernel, grid), out_shape=jax.Shape...]
where the time goes in v2:
time: 54.5 us; the launch traced here: 54.2 us
  Pallas kernels  52.6 us (97%)
  local copies, waits for them, and re-layouts  1.67 us (3%)
    pallas_call x1, Pallas kernels, fused(): pl.pallas_call(functools.partial(fused_kernel, grid), out_shape=jax.Shape...  52.6 us
    unnamed x1, local copies, waits for them, and re-layouts  1.67 us

profile of v2, /device:TPU:0, one launch (start us, length us, event | category | flops | bytes accessed | tf_op | source)
XLA Modules:
  0.0 54.2 jit_solution(5383361772426474202)
XLA Ops:
  0.0 52.6 %shard_map.109 = bf16[128,1024]{1,0:T(8,128)(2,1)} custom-call(bf16[128,1024]{1,0:T(8,128)(2,1)} %target.1, bf16[128,1024]{1,0:T(8,128)(2,1)} %source.1, bf16[2,4,1024]{2,1,0:T(4,128)(2,1)} %target_gains.1, bf16[2,1024]{1,0:T(2,128)(2,1)} %source_gain.1, bf16[2,1024,512]{2,1,0:T(8,128)(2,1)} %wq_hbm.1, bf16[2,1024,512]{2,1,0:T(8,128)(2,1)} %wk_hbm.1, ...), custom_call_target="tpu_custom_call" | custom-call | tf_op jit(solution)/shard_map/pallas_call | solution.py:526
  52.6 1.7 %copy.13 = bf16[128,1024]{1,0:T(8,128)(2,1)} copy(bf16[128,1024]{1,0:T(8,128)(2,1)} %shard_map.109) | data formatting | bytes 524288
